TPU v7x, 256 devices: a whole 4x4x8 slice. The times are simulated.
256 devices in a mesh: sp: 64 (over z, y, core), tp: 4 (over x).
Axes of the slice: x: 4, y: 4, z: 8, core: 2. Of those that a mesh axis runs over, the one named last changes fastest.
Arguments:
- gate_in: bfloat16 [32768, 2048], P('sp', 'tp'), may hold values from -6 to 6
- value_in: bfloat16 [32768, 2048], P('sp', 'tp'), may hold values from -6 to 6
- gate_out: bfloat16 [32768, 2048], P('sp', 'tp'), may hold values from -6 to 6
- conv_taps: float32 [3, 2048], P(None, 'tp'), may hold values from -3.5 to 3.5
- proj_weight: bfloat16 [2048, 2048], P('tp'), may hold values from -0.125 to 0.125
- residual: bfloat16 [32768, 2048], P(('sp', 'tp')), may hold values from -6 to 6
- norm_gain: float32 [2048], replicated, may hold values from 0.1 to 1.9
- routes: int32 [32768, 2], P('sp'), may hold values from 0 to 63, all different within a row; in each aligned block of 128 rows (0 to 127, 128 to 255, ...) at most 8 rows name the same one
- route_weight: float32 [32768, 2], P('sp'), may hold values from 0.1 to 0.9
- expert_gate: bfloat16 [64, 2048, 2048], P('sp', None, 'tp'), may hold values from -0.125 to 0.125
- expert_up: bfloat16 [64, 2048, 2048], P('sp', None, 'tp'), may hold values from -0.125 to 0.125
- expert_down: bfloat16 [64, 2048, 2048], P('sp', 'tp'), may hold values from -0.125 to 0.125
Outputs:
- layer_out: bfloat16 [32768, 2048], P(('sp', 'tp'))
Inputs may be any that keep to these rules, and one draw needn't show every extreme that they name: `routes`: A token's 2 experts differ. In each aligned block of 128 tokens no expert is named by more than 8 tokens, a bound that some block reaches.
All inputs are finite; a program needn't handle non-finite values.
Results may differ from a plain program's by a relative error of at most 0.012.
Values may be sent and summed in bfloat16 or wider, within the bound.
A program may use at most 128 MiB of HBM per device.

v0:
```python
import jax
import jax.numpy as jnp
from jax import lax
from jax.sharding import PartitionSpec as P


def gather_turned(arrays, axis, dims):
    turned = [jnp.moveaxis(a, dim, 0) for a, dim in zip(arrays, dims)]
    widths = [t[0].size for t in turned]
    both = jnp.concatenate([t.reshape(-1, w) for t, w in zip(turned, widths)], axis=1)
    result = lax.all_gather(both, axis, axis=0, tiled=True)
    parts = jnp.split(result, [sum(widths[:k]) for k in range(1, len(widths))], axis=1)
    return tuple(
        (
            jnp.moveaxis(b.reshape(-1, *t.shape[1:]), 0, dim)
            for b, t, dim in zip(parts, turned, dims)
        )
    )


def passed_along(shard, axis, by):
    size = lax.axis_size(axis)
    pairs = [(i, i + by) for i in range(size) if 0 <= i + by < size]
    return lax.ppermute(shard, axis, pairs)


def split_up(shard, dim, size):
    before, after = (shard.shape[:dim], shard.shape[dim + 1 :])
    return jnp.moveaxis(shard.reshape(*before, size, -1, *after), dim, 0)


def sum_at_owner(shard, axis, dim):
    parts = split_up(shard, dim, lax.axis_size(axis))
    arrived = lax.all_to_all(parts, axis, split_axis=0, concat_axis=0, tiled=True)
    return arrived.astype(jnp.float32).sum(axis=0)


def rounded(values):
    return lax.optimization_barrier(values.astype(jnp.bfloat16)).astype(jnp.float32)


def slot_numbers(route_ids, block_rows, expert_count):
    block_count = route_ids.shape[0] // block_rows
    flat_ids = route_ids.reshape(block_count, block_rows * route_ids.shape[1])
    one_hot = (
        flat_ids[:, :, None] == jnp.arange(expert_count, dtype=jnp.int32)[None, None, :]
    ).astype(jnp.int32)
    before = jnp.cumsum(one_hot, axis=1) - one_hot
    return jnp.sum(before * one_hot, axis=2).reshape(route_ids.shape)


def normalize(hidden_rows, norm_gain):
    inverse = lax.rsqrt(jnp.mean(hidden_rows * hidden_rows, axis=-1, keepdims=True) + 1e-05)
    return (hidden_rows * inverse * norm_gain).astype(jnp.bfloat16)


def dispatch_rows(normed, route_ids, block_rows, expert_count, capacity):
    row_count = route_ids.shape[0]
    top_count = route_ids.shape[1]
    block_count = row_count // block_rows
    slots = slot_numbers(route_ids, block_rows, expert_count)
    row_ids = jnp.arange(row_count, dtype=jnp.int32)
    flat_index = ((row_ids // block_rows)[:, None] * expert_count + route_ids) * capacity + slots
    slot_token = (
        jnp.full((block_count * expert_count * capacity,), row_count, jnp.int32)
        .at[flat_index.reshape(-1)]
        .set(jnp.repeat(row_ids, top_count))
    )
    padded_rows = jnp.concatenate([normed, jnp.zeros((1, normed.shape[1]), jnp.bfloat16)], axis=0)
    outgoing = padded_rows[slot_token].reshape(block_count, expert_count, capacity, normed.shape[1])
    return (outgoing, slots)


def body(
    gate_in,
    value_in,
    gate_out,
    conv_taps,
    proj_weight,
    residual,
    norm_gain,
    routes,
    route_weight,
    expert_gate,
    expert_up,
    expert_down,
):
    tok_dev = gate_in.shape[0]
    model_width = residual.shape[1]
    tp_count = lax.axis_size("tp")
    groups = lax.axis_size("sp")
    quarter = residual.shape[0]
    top_count = routes.shape[1]
    capacity = 2 * quarter * top_count // groups
    tp_index = lax.axis_index("tp")
    first_own = tp_index * quarter
    whole_gate, whole_up, whole_down = gather_turned(
        (expert_gate[0], expert_up[0], expert_down[0]), "tp", (1, 1, 0)
    )
    prior_gate, prior_value = passed_along(
        (gate_in[tok_dev - 2 :], value_in[tok_dev - 2 :]), "sp", 1
    )
    product = gate_in.astype(jnp.float32) * value_in.astype(jnp.float32)
    prior_mix = prior_gate.astype(jnp.float32) * prior_value.astype(jnp.float32)
    padded = jnp.concatenate([prior_mix, product], axis=0)
    conv_sum = conv_taps[0] * padded[:-2] + conv_taps[1] * padded[1:-1] + conv_taps[2] * padded[2:]
    mixed_out = (gate_out.astype(jnp.float32) * conv_sum).astype(jnp.bfloat16)
    own_routes = lax.dynamic_slice_in_dim(routes, first_own, quarter, 0)
    own_weights = lax.dynamic_slice_in_dim(route_weight, first_own, quarter, 0)
    summed = sum_at_owner(
        rounded(jnp.dot(mixed_out, proj_weight, preferred_element_type=jnp.float32)).astype(
            jnp.bfloat16
        ),
        "tp",
        0,
    )
    my_rows = residual.astype(jnp.float32) + summed
    normed = normalize(my_rows, norm_gain)
    outgoing, own_slots = dispatch_rows(normed, own_routes, quarter, groups, capacity)
    own_arrived = lax.all_to_all(outgoing, "sp", split_axis=1, concat_axis=1, tiled=True)
    own_flat = own_arrived.reshape(groups * capacity, model_width)
    gate_pre = jnp.dot(own_flat, whole_gate, preferred_element_type=jnp.float32)
    up_pre = jnp.dot(own_flat, whole_up, preferred_element_type=jnp.float32)
    hidden = (jax.nn.silu(gate_pre) * up_pre).astype(jnp.bfloat16)
    hidden_width = hidden.shape[1] // tp_count
    partial_sum = jnp.zeros((groups * capacity, model_width), jnp.float32)
    for group in range(tp_count):
        lower = group * hidden_width
        partial_sum = partial_sum + rounded(
            jnp.dot(
                hidden[:, lower : lower + hidden_width],
                whole_down[lower : lower + hidden_width],
                preferred_element_type=jnp.float32,
            )
        )
    expert_rows = partial_sum.astype(jnp.bfloat16)
    returned = lax.all_to_all(
        expert_rows.reshape(groups, capacity, model_width),
        "sp",
        split_axis=0,
        concat_axis=0,
        tiled=True,
    )
    flat_pick = own_routes * capacity + own_slots
    picked = returned.reshape(groups * capacity, model_width)[flat_pick]
    weighted = jnp.sum(own_weights[:, :, None] * picked.astype(jnp.float32), axis=1)
    return (my_rows + weighted).astype(jnp.bfloat16)


def solution(mesh):
    placed = (
        P("sp", "tp"),
        P("sp", "tp"),
        P("sp", "tp"),
        P(None, "tp"),
        P("tp", None),
        P(("sp", "tp"), None),
        P(),
        P("sp", None),
        P("sp", None),
        P("sp", None, "tp"),
        P("sp", None, "tp"),
        P("sp", "tp", None),
    )
    return jax.shard_map(
        body, mesh=mesh, in_specs=placed, out_specs=P(("sp", "tp"), None), check_vma=False
    )
```

profile of v0, /device:TPU:1, one launch (start us, length us, event | category | flops | bytes accessed | tf_op | source)
XLA Modules:
  0.0 378.2 jit_solution(1630684315032256582)
XLA Ops:
  6.5 4.1 %copy.29 = bf16[1,2048,512]{1,2,0:T(8,128)(2,1)} copy(bf16[1,2048,512]{2,1,0:T(8,128)(2,1)} %param.21) | data formatting | bytes 4194304 | tf_op args[9]
  10.7 4.0 %copy.30 = bf16[1,2048,512]{1,2,0:T(8,128)(2,1)} copy(bf16[1,2048,512]{2,1,0:T(8,128)(2,1)} %param.22) | data formatting | bytes 4194304 | tf_op args[10]
  14.6 6.4 %pad_maximum_fusion = bf16[512,6144]{1,0:T(8,128)(2,1)} fusion(bf16[512,2048]{1,0:T(8,128)(2,1)} %bitcast.43, bf16[512,2048]{1,0:T(8,128)(2,1)} %bitcast.41, bf16[512,2048]{1,0:T(8,128)(2,1)} %bitcast.40), kind=kLoop, calls=%fused_computation.7 | loop fusion | flops 18874368 | bytes 12582912 | tf_op jit(solution)/shard_map/concatenate | solution.py:10
  21.1 0.7 slice.56
  21.8 4.6 %collective-permute-start = (bf16[2,512]{1,0:T(2,128)(2,1)S(1)}, bf16[2,512]{1,0:T(2,128)(2,1)S(1)}, u32[]{:S(2)}, u32[]{:S(2)}) collective-permute-start(bf16[2,512]{1,0:T(2,128)(2,1)S(1)} %slice.56), channel_id=1, source_target_pairs={{0,4},{4,8},{8,12},{12,16},{16,20},{20,24},{24,28},{28,32},{32,36}... | collective-permute-start | bytes 6152 | tf_op jit(solution)/shard_map/ppermute | solution.py:24
  26.4 0.7 slice.57
  27.1 1.9 collective-permute-start.1
  29.0 1.3 convert_multiply_fusion
  30.4 0.7 constant_dynamic-slice_fusion
  31.4 3.8 %convolution_convert_fusion.4 = bf16[512,2048]{1,0:T(8,128)(2,1)} fusion(bf16[512,2048]{1,0:T(8,128)(2,1)S(1)} %copy-done, f32[2,512]{1,0:T(2,128)S(1)} %convert_multiply_fusion.1, f32[512,512]{1,0:T(8,128)S(1)} %convert_multiply_fusion, bf16[512,512]{1,0:T(8,128)(2,1)} %param.14, f32[512]{0:T(512)S(1)} %bitcast.49, f32[512]{0:T(512)S(1)} %bitcast.50, ...), kind=kOutput, calls=%fused_computation.15 | convolution fusion | flops 1077411840 | bytes 5777408 | tf_op jit(solution)/shard_map/dot_general | solution.py:111
  35.2 4.0 %all-to-all-start = ((bf16[4,128,2048]{2,1,0:T(8,128)(2,1)}), bf16[4,128,2048]{2,1,0:T(8,128)(2,1)S(1)}, u32[]{:S(2)}, u32[]{:S(2)}) async-start(bf16[4,128,2048]{2,1,0:T(8,128)(2,1)} %bitcast.42), calls=%async_computation | async-start | bytes 4194304 | tf_op jit(solution)/shard_map/all_to_all | solution.py:34
  39.2 0.6 reduce-window.6
  41.1 1.4 scatter_custom_fusion
  42.5 37.7 %all-to-all-done = bf16[4,128,2048]{2,1,0:T(8,128)(2,1)S(1)} async-done(((bf16[4,128,2048]{2,1,0:T(8,128)(2,1)}), bf16[4,128,2048]{2,1,0:T(8,128)(2,1)S(1)}, u32[]{:S(2)}, u32[]{:S(2)}) %all-to-all-start) | async-done | bytes 2097184 | tf_op jit(solution)/shard_map/all_to_all | solution.py:34
  80.7 1.3 multiply_reduce_fusion.1
  82.2 3.3 gather_fusion
  85.5 66.6 %all_to_all.15 = bf16[1,64,8,2048]{3,2,0,1:T(8,128)(2,1)S(1)} all-to-all(bf16[1,64,8,2048]{3,2,0,1:T(8,128)(2,1)} %bitcast.39), channel_id=1, replica_groups=mesh['sp'=64,'tp'=4] {'sp'}, dimensions={1} | all-to-all | bytes 4194304 | tf_op jit(solution)/shard_map/all_to_all | solution.py:120
  152.1 116.1 %all-gather.2.cloned.1.call-done = bf16[2048,6144]{1,0:T(8,128)(2,1)} async-done(((bf16[512,6144]{1,0:T(8,128)(2,1)}), bf16[2048,6144]{1,0:T(8,128)(2,1)}) %all-gather.2.cloned.1.call-update) | async-done | bytes 25165840 | tf_op jit(solution)/shard_map/all_gather | solution.py:11
  268.2 6.9 %fusion.2 = f32[512,2048]{1,0:T(8,128)S(1)} fusion(bf16[2048,6144]{1,0:T(8,128)(2,1)} %all-gather.2.cloned.1.call-done, bf16[1,64,8,2048]{3,2,0,1:T(8,128)(2,1)S(1)} %all_to_all.15), kind=kOutput, calls=%fused_computation.5 | convolution fusion | flops 4294967296 | bytes 14680064 | tf_op jit(solution)/shard_map/dot_general | solution.py:122
  275.2 8.2 %multiply_convert_fusion = bf16[512,2048]{1,0:T(8,128)(2,1)S(1)} fusion(f32[512,2048]{1,0:T(8,128)S(1)} %fusion.2, bf16[2048,6144]{1,0:T(8,128)(2,1)} %all-gather.2.cloned.1.call-done, bf16[1,64,8,2048]{3,2,0,1:T(8,128)(2,1)S(1)} %all_to_all.15), kind=kOutput, calls=%fused_computation.9 | convolution fusion | flops 4301258752 | bytes 16777216 | tf_op jit(solution)/shard_map/dot_general | solution.py:123
  283.4 2.9 convolution_convert_fusion.3
  286.3 2.9 convolution_convert_fusion.2
  289.1 2.9 convolution_convert_fusion.1
  292.0 2.9 convolution_convert_fusion
  294.9 3.1 fusion.6
  298.0 11.9 %all-to-all-start.2 = ((bf16[64,8,2048]{2,1,0:T(8,128)(2,1)}), bf16[64,8,2048]{2,1,0:T(8,128)(2,1)S(1)}, u32[]{:S(2)}, u32[]{:S(2)}) async-start(bf16[64,8,2048]{2,1,0:T(8,128)(2,1)} %fusion.6), calls=%async_computation.2 | async-start | bytes 4194304 | tf_op jit(solution)/shard_map/all_to_all | solution.py:137
  310.1 0.7 constant_dynamic-slice_fusion.1
  310.9 48.8 %all-to-all-done.2 = bf16[64,8,2048]{2,1,0:T(8,128)(2,1)S(1)} async-done(((bf16[64,8,2048]{2,1,0:T(8,128)(2,1)}), bf16[64,8,2048]{2,1,0:T(8,128)(2,1)S(1)}, u32[]{:S(2)}, u32[]{:S(2)}) %all-to-all-start.2) | async-done | bytes 2097184 | tf_op jit(solution)/shard_map/all_to_all | solution.py:137
  359.7 2.3 gather_fusion.1
  362.0 3.4 reshape.233
  365.4 5.0 %multiply_reduce_fusion = f32[128,2048]{1,0:T(8,128)S(1)} fusion(f32[128,2,2048]{2,1,0:T(2,128)} %reshape.233, f32[128,2]{1,0:T(8,128)S(1)} %copy.23), kind=kLoop, calls=%fused_computation.23 | loop fusion | flops 786432 | bytes 3146752 | tf_op jit(solution)/shard_map/reduce_sum | solution.py:146
  370.4 1.0 add_convert_fusion.1
  (45 shorter events, 2.4 us)
Async XLA Ops:
  6.5 24.8 %copy-start = (bf16[512,2048]{1,0:T(8,128)(2,1)S(1)}, bf16[512,2048]{1,0:T(8,128)(2,1)}, u32[]{:S(2)}) copy-start(bf16[512,2048]{1,0:T(8,128)(2,1)} %param.16) | copy-start | bytes 6291460
  6.5 261.7 %all-gather.2.cloned.1.call-start = ((), (), s32[]{:S(2)}) async-start(), calls=%async_computation.3 | async-start | bytes 31457280 | tf_op jit(solution)/shard_map/all_gather | solution.py:11
  21.1 7.9 %copy-start.5 = (f32[3,512]{1,0:T(4,128)S(1)}, f32[3,512]{1,0:T(4,128)}, u32[]{:S(2)}) copy-start(f32[3,512]{1,0:T(4,128)} %param.15) | copy-start | bytes 18436
  21.8 9.5 %collective-permute-start = (bf16[2,512]{1,0:T(2,128)(2,1)S(1)}, bf16[2,512]{1,0:T(2,128)(2,1)S(1)}, u32[]{:S(2)}, u32[]{:S(2)}) collective-permute-start(bf16[2,512]{1,0:T(2,128)(2,1)S(1)} %slice.56), channel_id=1, source_target_pairs={{0,4},{4,8},{8,12},{12,16},{16,20},{20,24},{24,28},{28,32},{32,36}... | collective-permute-start | bytes 6152 | tf_op jit(solution)/shard_map/ppermute | solution.py:24
  27.1 4.3 %collective-permute-start.1 = (bf16[2,512]{1,0:T(2,128)(2,1)S(1)}, bf16[2,512]{1,0:T(2,128)(2,1)S(1)}, u32[]{:S(2)}, u32[]{:S(2)}) collective-permute-start(bf16[2,512]{1,0:T(2,128)(2,1)S(1)} %slice.57), channel_id=1, source_target_pairs={{0,4},{4,8},{8,12},{12,16},{16,20},{20,24},{24,28},{28,32},{32,36}... | collective-permute-start | bytes 6152 | tf_op jit(solution)/shard_map/ppermute | solution.py:24
  35.2 45.1 %all-to-all-start = ((bf16[4,128,2048]{2,1,0:T(8,128)(2,1)}), bf16[4,128,2048]{2,1,0:T(8,128)(2,1)S(1)}, u32[]{:S(2)}, u32[]{:S(2)}) async-start(bf16[4,128,2048]{2,1,0:T(8,128)(2,1)} %bitcast.42), calls=%async_computation | async-start | bytes 4194304 | tf_op jit(solution)/shard_map/all_to_all | solution.py:34
  42.5 39.4 %copy-start.4 = (f32[2048]{0:T(1024)S(1)}, f32[2048]{0:T(1024)}, u32[]{:S(2)}) copy-start(f32[2048]{0:T(1024)} %param.18) | copy-start | bytes 24580
  80.3 1.7 copy-start.2
  298.0 61.6 %all-to-all-start.2 = ((bf16[64,8,2048]{2,1,0:T(8,128)(2,1)}), bf16[64,8,2048]{2,1,0:T(8,128)(2,1)S(1)}, u32[]{:S(2)}, u32[]{:S(2)}) async-start(bf16[64,8,2048]{2,1,0:T(8,128)(2,1)} %fusion.6), calls=%async_computation.2 | async-start | bytes 4194304 | tf_op jit(solution)/shard_map/all_to_all | solution.py:137
  365.4 5.0 %copy-start.3 = (bf16[128,2048]{1,0:T(8,128)(2,1)S(1)}, bf16[128,2048]{1,0:T(8,128)(2,1)}, u32[]{:S(2)}) copy-start(bf16[128,2048]{1,0:T(8,128)(2,1)} %param.17) | copy-start | bytes 1572868
  365.4 6.0 %copy-start.1 = (bf16[512,2048]{1,0:T(8,128)(2,1)S(1)}, bf16[512,2048]{1,0:T(8,128)(2,1)}, u32[]{:S(2)}) copy-start(bf16[512,2048]{1,0:T(8,128)(2,1)} %param.16) | copy-start | bytes 6291460
Sparse Core Ops, SparseCore 0:
  21.2 246.9 all-gather.1
where the time goes:
time: 380 us; the launch traced here: 378 us
  waiting for transfers between devices  203 us (53%)
  blocking collectives  66.6 us (18%)
  matrix products  30.4 us (8%)
  local copies, waits for them, and re-layouts  22.8 us (6%)
  starting transfers between devices  22.4 us (6%)
  other arithmetic  19.7 us (5%)
  between operations  13.7 us (4%)
    all_gather x1, waiting for transfers between devices, gather_turned(): result = lax.all_gather(both, axis, axis=0, tiled=True)  116 us
    all_to_all x1, blocking collectives, body(): lax.all_to_all(outgoing, 'sp', split_axis=1, concat_axis=1, tiled=True)  66.6 us
    all_to_all x1, waiting for transfers between devices, body(): lax.all_to_all(expert_rows.reshape(groups, capacity, model_width), 'sp',...  48.8 us
    all_to_all x1, waiting for transfers between devices, sum_at_owner(): lax.all_to_all(parts, axis, split_axis=0, concat_axis=0, tiled=True)  37.7 us
    all_to_all x1, starting transfers between devices, body(): lax.all_to_all(expert_rows.reshape(groups, capacity, model_width), 'sp',...  11.9 us
    dot_general x4, matrix products, body(): jnp.dot(hidden[:, lower:lower + hidden_width], whole_down[lower:lower + h...  11.5 us
    unnamed x15, local copies, waits for them, and re-layouts  8.24 us
    dot_general x1, matrix products, body(): up_pre = jnp.dot(own_flat, whole_up, preferred_element_type=jnp.float32)  8.24 us
  transfers between devices with their start and end apart: 5, of which 3 were waited for; matrix products, arithmetic and copies ran while one was open for 4% of the time, Pallas kernels for 0%

commit v1 on v0

--- a/solution.py
+++ b/solution.py
@@ -4,18 +4,14 @@
 from jax.sharding import PartitionSpec as P
 
 
-def gather_turned(arrays, axis, dims):
-    turned = [jnp.moveaxis(a, dim, 0) for a, dim in zip(arrays, dims)]
-    widths = [t[0].size for t in turned]
-    both = jnp.concatenate([t.reshape(-1, w) for t, w in zip(turned, widths)], axis=1)
-    result = lax.all_gather(both, axis, axis=0, tiled=True)
-    parts = jnp.split(result, [sum(widths[:k]) for k in range(1, len(widths))], axis=1)
-    return tuple(
-        (
-            jnp.moveaxis(b.reshape(-1, *t.shape[1:]), 0, dim)
-            for b, t, dim in zip(parts, turned, dims)
-        )
-    )
+def swapped(shard, first):
+    sp_count, tp_count = lax.axis_size("sp"), lax.axis_size("tp")
+    pairs = []
+    for s in range(sp_count):
+        for t in range(tp_count):
+            other = t ^ 1 if (s % 2 == 0) == first else tp_count - 1 - t
+            pairs.append((s * tp_count + t, s * tp_count + other))
+    return lax.ppermute(shard, ("sp", "tp"), pairs)
 
 
 def passed_along(shard, axis, by):
@@ -94,9 +90,9 @@
     capacity = 2 * quarter * top_count // groups
     tp_index = lax.axis_index("tp")
     first_own = tp_index * quarter
-    whole_gate, whole_up, whole_down = gather_turned(
-        (expert_gate[0], expert_up[0], expert_down[0]), "tp", (1, 1, 0)
-    )
+    gates = (expert_gate[0], swapped(expert_gate[0], True))
+    ups = (expert_up[0], swapped(expert_up[0], True))
+    downs = (expert_down[0], swapped(expert_down[0], True))
     prior_gate, prior_value = passed_along(
         (gate_in[tok_dev - 2 :], value_in[tok_dev - 2 :]), "sp", 1
     )
@@ -119,21 +115,24 @@
     outgoing, own_slots = dispatch_rows(normed, own_routes, quarter, groups, capacity)
     own_arrived = lax.all_to_all(outgoing, "sp", split_axis=1, concat_axis=1, tiled=True)
     own_flat = own_arrived.reshape(groups * capacity, model_width)
-    gate_pre = jnp.dot(own_flat, whole_gate, preferred_element_type=jnp.float32)
-    up_pre = jnp.dot(own_flat, whole_up, preferred_element_type=jnp.float32)
-    hidden = (jax.nn.silu(gate_pre) * up_pre).astype(jnp.bfloat16)
-    hidden_width = hidden.shape[1] // tp_count
-    partial_sum = jnp.zeros((groups * capacity, model_width), jnp.float32)
-    for group in range(tp_count):
-        lower = group * hidden_width
-        partial_sum = partial_sum + rounded(
-            jnp.dot(
-                hidden[:, lower : lower + hidden_width],
-                whole_down[lower : lower + hidden_width],
-                preferred_element_type=jnp.float32,
-            )
-        )
-    expert_rows = partial_sum.astype(jnp.bfloat16)
+    other_flat = swapped(own_flat, False)
+
+    def hidden_of(rows):
+        hidden = []
+        for gate, up in zip(gates, ups):
+            gate_pre = jnp.dot(rows, gate, preferred_element_type=jnp.float32)
+            up_pre = jnp.dot(rows, up, preferred_element_type=jnp.float32)
+            hidden.append((jax.nn.silu(gate_pre) * up_pre).astype(jnp.bfloat16))
+        return hidden
+
+    def down_of(hidden):
+        total = jnp.dot(hidden[0], downs[0], preferred_element_type=jnp.float32)
+        return total + jnp.dot(hidden[1], downs[1], preferred_element_type=jnp.float32)
+
+    own_hidden = hidden_of(own_flat)
+    other_partial = down_of(hidden_of(other_flat)).astype(jnp.bfloat16)
+    arrived_partial = swapped(other_partial, False)
+    expert_rows = (down_of(own_hidden) + arrived_partial.astype(jnp.float32)).astype(jnp.bfloat16)
     returned = lax.all_to_all(
         expert_rows.reshape(groups, capacity, model_width),
         "sp",

time: 380 us -> 322 us (0.85)
  waiting for transfers between devices: 203 us -> 150 us
  matrix products: 30.4 us -> 47.5 us
  between operations: 13.7 us -> 0.28 us
  blocking collectives: 66.6 us -> 62.5 us
    all_gather x1 -> x0, waiting for transfers between devices: 116 us -> none  [gather_turned(): result = lax.all_gather(both, axis, axis=0, tiled=True)]
    ppermute x0 -> x5, waiting for transfers between devices: none -> 78.8 us  [swapped(): return lax.ppermute(shard, ('sp', 'tp'), pairs)]
    dot_general x6 -> x8, matrix products: 26.6 us -> 43.7 us  [the longest x2 15.7 us: down_of(): jnp.dot(hidden[1], downs[1], preferred_element_type=jnp.float32)]
    all_to_all x1, waiting for transfers between devices: 37.7 us -> 22.7 us  [sum_at_owner(): lax.all_to_all(parts, axis, split_axis=0, concat_axis=0, tiled=True)]
    concatenate x1 -> x0, other arithmetic: 6.45 us -> none  [gather_turned(): jnp.concatenate([t.reshape(-1, w) for t, w in zip(turned, widths)], axis=1)]
    unnamed x15 -> x23, local copies, waits for them, and re-layouts: 8.24 us -> 3.52 us
    all_to_all x1, starting transfers between devices: 11.9 us -> 7.62 us  [body(): lax.all_to_all(expert_rows.reshape(groups, capacity, model_width), 'sp',...]
    all_to_all x1, blocking collectives: 66.6 us -> 62.5 us  [body(): lax.all_to_all(outgoing, 'sp', split_axis=1, concat_axis=1, tiled=True)]
  transfers between devices with their start and end apart: 5 -> 9, of which waited for: 3 -> 7; matrix products, arithmetic and copies ran while one was open for 4% -> 13% of each run, Pallas kernels for 0% -> 0%
where the time goes in v1:
time: 322 us; the launch traced here: 321 us
  waiting for transfers between devices  150 us (47%)
  blocking collectives  62.5 us (19%)
  matrix products  47.5 us (15%)
  starting transfers between devices  22.1 us (7%)
  local copies, waits for them, and re-layouts  21.1 us (7%)
  other arithmetic  17.4 us (5%)
    ppermute x5, waiting for transfers between devices, swapped(): return lax.ppermute(shard, ('sp', 'tp'), pairs)  78.8 us
    all_to_all x1, blocking collectives, body(): lax.all_to_all(outgoing, 'sp', split_axis=1, concat_axis=1, tiled=True)  62.5 us
    all_to_all x1, waiting for transfers between devices, body(): lax.all_to_all(expert_rows.reshape(groups, capacity, model_width), 'sp',...  48.7 us
    all_to_all x1, waiting for transfers between devices, sum_at_owner(): lax.all_to_all(parts, axis, split_axis=0, concat_axis=0, tiled=True)  22.7 us
    dot_general x2, matrix products, down_of(): jnp.dot(hidden[1], downs[1], preferred_element_type=jnp.float32)  15.7 us
    dot_general x2, matrix products, down_of(): total = jnp.dot(hidden[0], downs[0], preferred_element_type=jnp.float32)  15.1 us
    dot_general x3, matrix products, hidden_of(): gate_pre = jnp.dot(rows, gate, preferred_element_type=jnp.float32)  9.12 us
    all_to_all x1, starting transfers between devices, body(): lax.all_to_all(expert_rows.reshape(groups, capacity, model_width), 'sp',...  7.62 us
  transfers between devices with their start and end apart: 9, of which 7 were waited for; matrix products, arithmetic and copies ran while one was open for 13% of the time, Pallas kernels for 0%

profile of v1, /device:TPU:1, one launch (start us, length us, event | category | flops | bytes accessed | tf_op | source)
XLA Modules:
  0.0 321.1 jit_solution(9930334532394653648)
XLA Ops:
  0.9 4.6 %collective-permute-start.1 = (bf16[2,512]{1,0:T(2,128)(2,1)S(1)}, bf16[2,512]{1,0:T(2,128)(2,1)S(1)}, u32[]{:S(2)}, u32[]{:S(2)}) collective-permute-start(bf16[2,512]{1,0:T(2,128)(2,1)S(1)} %slice.29), channel_id=1, source_target_pairs={{0,4},{4,8},{8,12},{12,16},{16,20},{20,24},{24,28},{28,32},{32,36}... | collective-permute-start | bytes 6152 | tf_op jit(solution)/shard_map/ppermute | solution.py:20
  6.2 1.9 collective-permute-start
  8.1 1.3 convert_multiply_fusion
  10.4 3.8 %convolution_convert_fusion = bf16[512,2048]{1,0:T(8,128)(2,1)} fusion(bf16[512,2048]{1,0:T(8,128)(2,1)S(1)} %copy-done, f32[2,512]{1,0:T(2,128)S(1)} %convert_multiply_fusion.1, f32[512,512]{1,0:T(8,128)S(1)} %convert_multiply_fusion, bf16[512,512]{1,0:T(8,128)(2,1)} %param.14, f32[512]{0:T(512)S(1)} %bitcast.78, f32[512]{0:T(512)S(1)} %bitcast.79, ...), kind=kOutput, calls=%fused_computation.6 | convolution fusion | flops 1077411840 | bytes 5777408 | tf_op jit(solution)/shard_map/dot_general | solution.py:107
  14.2 4.4 %all-to-all-start = ((bf16[4,128,2048]{2,1,0:T(8,128)(2,1)}), bf16[4,128,2048]{2,1,0:T(8,128)(2,1)}, u32[]{:S(2)}, u32[]{:S(2)}) async-start(bf16[4,128,2048]{2,1,0:T(8,128)(2,1)} %bitcast.71), calls=%async_computation | async-start | bytes 4194304 | tf_op jit(solution)/shard_map/all_to_all | solution.py:30
  20.6 1.4 scatter_custom_fusion
  22.0 22.7 %all-to-all-done = bf16[4,128,2048]{2,1,0:T(8,128)(2,1)} async-done(((bf16[4,128,2048]{2,1,0:T(8,128)(2,1)}), bf16[4,128,2048]{2,1,0:T(8,128)(2,1)}, u32[]{:S(2)}, u32[]{:S(2)}) %all-to-all-start) | async-done | bytes 2097184 | tf_op jit(solution)/shard_map/all_to_all | solution.py:30
  44.7 2.1 convert_reduce_fusion
  48.0 3.3 %gather_fusion = bf16[512,2048]{1,0:T(8,128)(2,1)} fusion(bf16[129,2048]{1,0:T(8,128)(2,1)S(1)} %concatenate.7, s32[1024]{0:T(1024)S(1)} %pad_clamp_fusion.1), kind=kCustom, calls=%fused_computation | custom fusion | bytes 4196352 | tf_op jit(solution)/shard_map/gather | solution.py:66
  51.4 62.5 %all_to_all.15 = bf16[1,64,8,2048]{3,2,0,1:T(8,128)(2,1)S(1)} all-to-all(bf16[1,64,8,2048]{3,2,0,1:T(8,128)(2,1)} %bitcast.70), channel_id=1, replica_groups=mesh['sp'=64,'tp'=4] {'sp'}, dimensions={1} | all-to-all | bytes 4194304 | tf_op jit(solution)/shard_map/all_to_all | solution.py:116
  113.9 1.3 copy-done.4
  116.1 2.1 collective-permute-start.4
  118.8 40.4 %collective-permute-done.5 = bf16[512,2048]{1,0:T(8,128)(2,1)S(1)} collective-permute-done((bf16[512,2048]{1,0:T(8,128)(2,1)S(1)}, bf16[512,2048]{1,0:T(8,128)(2,1)S(1)}, u32[]{:S(2)}, u32[]{:S(2)}) %collective-permute-start.5) | collective-permute-done | bytes 2097184 | tf_op jit(solution)/shard_map/ppermute | solution.py:14
  159.1 2.3 fusion.35
  162.1 1.3 copy-done.9
  163.4 2.2 fusion.57
  165.7 7.5 %fusion.11 = f32[512,2048]{1,0:T(8,128)} fusion(f32[512,512]{1,0:T(8,128)} %fusion.35, bf16[1,512,2048]{2,1,0:T(8,128)(2,1)} %param.23, bf16[512,2048]{1,0:T(8,128)(2,1)} %copy-done.10, bf16[1,2048,512]{2,1,0:T(8,128)(2,1)} %param.22), kind=kOutput, calls=%fused_computation.31 | convolution fusion | flops 2149056512 | bytes 11534336 | tf_op jit(solution)/shard_map/dot_general | solution.py:129
  173.2 13.4 %collective-permute-done.4 = bf16[512,2048]{1,0:T(8,128)(2,1)} collective-permute-done((bf16[512,2048]{1,0:T(8,128)(2,1)}, bf16[512,2048]{1,0:T(8,128)(2,1)}, u32[]{:S(2)}, u32[]{:S(2)}) %collective-permute-start.4) | collective-permute-done | bytes 2097184 | tf_op jit(solution)/shard_map/ppermute | solution.py:14
  186.6 22.5 %collective-permute-done.3 = bf16[2048,512]{1,0:T(8,128)(2,1)} collective-permute-done((bf16[2048,512]{1,0:T(8,128)(2,1)}, bf16[2048,512]{1,0:T(8,128)(2,1)}, u32[]{:S(2)}, u32[]{:S(2)}) %collective-permute-start.3) | collective-permute-done | bytes 2097184 | tf_op jit(solution)/shard_map/ppermute | solution.py:14
  209.1 8.1 %add_convert_fusion.1 = bf16[512,2048]{1,0:T(8,128)(2,1)} fusion(f32[512,2048]{1,0:T(8,128)} %fusion.11, bf16[512,2048]{1,0:T(8,128)(2,1)} %collective-permute-done.4, f32[512,512]{1,0:T(8,128)} %fusion.57, bf16[512,2048]{1,0:T(8,128)(2,1)} %copy-done.10, bf16[2048,512]{1,0:T(8,128)(2,1)} %collective-permute-done.3), kind=kOutput, calls=%fused_computation.4 | convolution fusion | flops 2151153664 | bytes 13631488 | tf_op jit(solution)/shard_map/dot_general | solution.py:130
  217.2 4.6 %fusion.37 = f32[512,512]{1,0:T(8,128)} fusion(bf16[1,2048,512]{2,1,0:T(8,128)(2,1)} %param.21, bf16[1,64,8,2048]{3,2,0,1:T(8,128)(2,1)} %copy-done.4), kind=kOutput, calls=%fused_computation.70 | convolution fusion | flops 1073741824 | bytes 5242880 | tf_op jit(solution)/shard_map/dot_general | solution.py:123
  221.8 3.8 %fusion.39 = f32[512,512]{1,0:T(8,128)} fusion(bf16[2048,512]{1,0:T(8,128)(2,1)} %collective-permute-done.3, bf16[1,64,8,2048]{3,2,0,1:T(8,128)(2,1)S(1)} %copy-done.5), kind=kOutput, calls=%fused_computation.72 | convolution fusion | flops 1073741824 | bytes 5242880 | tf_op jit(solution)/shard_map/dot_general | solution.py:124
  225.7 7.5 %fusion.9 = f32[512,2048]{1,0:T(8,128)} fusion(f32[512,512]{1,0:T(8,128)} %fusion.37, bf16[1,512,2048]{2,1,0:T(8,128)(2,1)} %param.23, bf16[1,2048,512]{2,1,0:T(8,128)(2,1)} %param.22, bf16[1,64,8,2048]{3,2,0,1:T(8,128)(2,1)} %copy-done.4), kind=kOutput, calls=%fused_computation.29 | convolution fusion | flops 2149056512 | bytes 11534336 | tf_op jit(solution)/shard_map/dot_general | solution.py:129
  233.2 7.6 %fusion.10 = f32[512,2048]{1,0:T(8,128)} fusion(bf16[512,2048]{1,0:T(8,128)(2,1)} %collective-permute-done.4, f32[512,512]{1,0:T(8,128)} %fusion.39, bf16[2048,512]{1,0:T(8,128)(2,1)} %copy-done.9, bf16[1,64,8,2048]{3,2,0,1:T(8,128)(2,1)} %copy-done.4), kind=kOutput, calls=%fused_computation.30 | convolution fusion | flops 2149056512 | bytes 11534336 | tf_op jit(solution)/shard_map/dot_general | solution.py:130
  240.8 1.9 collective-permute-done.6
  242.7 6.6 %fusion = bf16[64,8,2048]{2,1,0:T(8,128)(2,1)} fusion(bf16[512,2048]{1,0:T(8,128)(2,1)} %collective-permute-done.6, f32[512,2048]{1,0:T(8,128)} %fusion.9, f32[512,2048]{1,0:T(8,128)} %fusion.10), kind=kLoop, calls=%fused_computation.7 | loop fusion | flops 4194304 | bytes 12582912 | tf_op jit(solution)/shard_map/reshape | solution.py:137
  249.4 7.6 %all-to-all-start.2 = ((bf16[64,8,2048]{2,1,0:T(8,128)(2,1)}), bf16[64,8,2048]{2,1,0:T(8,128)(2,1)}, u32[]{:S(2)}, u32[]{:S(2)}) async-start(bf16[64,8,2048]{2,1,0:T(8,128)(2,1)} %fusion), calls=%async_computation.2 | async-start | bytes 4194304 | tf_op jit(solution)/shard_map/all_to_all | solution.py:136
  257.9 48.7 %all-to-all-done.2 = bf16[64,8,2048]{2,1,0:T(8,128)(2,1)} async-done(((bf16[64,8,2048]{2,1,0:T(8,128)(2,1)}), bf16[64,8,2048]{2,1,0:T(8,128)(2,1)}, u32[]{:S(2)}, u32[]{:S(2)}) %all-to-all-start.2) | async-done | bytes 2097184 | tf_op jit(solution)/shard_map/all_to_all | solution.py:136
  306.6 5.2 %gather_fusion.1 = bf16[256,2048]{1,0:T(8,128)(2,1)} fusion(bf16[512,2048]{1,0:T(8,128)(2,1)} %bitcast.18, s32[1024]{0:T(1024)S(1)} %pad_clamp_fusion), kind=kCustom, calls=%fused_computation.1 | custom fusion | bytes 2098176 | tf_op jit(solution)/shard_map/gather | solution.py:144
  311.8 3.4 %reshape.233 = f32[128,2,2048]{2,1,0:T(2,128)} reshape(bf16[256,2048]{1,0:T(8,128)(2,1)} %gather_fusion.1) | data formatting | bytes 3145728 | tf_op jit(solution)/shard_map/convert_element_type | solution.py:145
  315.2 4.9 %multiply_reduce_fusion = f32[128,2048]{1,0:T(8,128)S(1)} fusion(f32[128,2,2048]{2,1,0:T(2,128)} %reshape.233, f32[128,2]{1,0:T(8,128)S(1)} %copy.19), kind=kLoop, calls=%fused_computation.8 | loop fusion | flops 786432 | bytes 3146752 | tf_op jit(solution)/shard_map/reduce_sum | solution.py:145
  320.1 1.0 add_convert_fusion.2
  (61 shorter events, 8.8 us)
Async XLA Ops:
  0.0 10.4 %copy-start = (bf16[512,2048]{1,0:T(8,128)(2,1)S(1)}, bf16[512,2048]{1,0:T(8,128)(2,1)}, u32[]{:S(2)}) copy-start(bf16[512,2048]{1,0:T(8,128)(2,1)} %param.16) | copy-start | bytes 6291460
  0.0 9.4 %copy-start.7 = (f32[3,512]{1,0:T(4,128)S(1)}, f32[3,512]{1,0:T(4,128)}, u32[]{:S(2)}) copy-start(f32[3,512]{1,0:T(4,128)} %param.15) | copy-start | bytes 18436
  0.9 9.5 %collective-permute-start.1 = (bf16[2,512]{1,0:T(2,128)(2,1)S(1)}, bf16[2,512]{1,0:T(2,128)(2,1)S(1)}, u32[]{:S(2)}, u32[]{:S(2)}) collective-permute-start(bf16[2,512]{1,0:T(2,128)(2,1)S(1)} %slice.29), channel_id=1, source_target_pairs={{0,4},{4,8},{8,12},{12,16},{16,20},{20,24},{24,28},{28,32},{32,36}... | collective-permute-start | bytes 6152 | tf_op jit(solution)/shard_map/ppermute | solution.py:20
  6.2 4.3 %collective-permute-start = (bf16[2,512]{1,0:T(2,128)(2,1)S(1)}, bf16[2,512]{1,0:T(2,128)(2,1)S(1)}, u32[]{:S(2)}, u32[]{:S(2)}) collective-permute-start(bf16[2,512]{1,0:T(2,128)(2,1)S(1)} %slice.28), channel_id=1, source_target_pairs={{0,4},{4,8},{8,12},{12,16},{16,20},{20,24},{24,28},{28,32},{32,36}... | collective-permute-start | bytes 6152 | tf_op jit(solution)/shard_map/ppermute | solution.py:20
  14.2 30.4 %all-to-all-start = ((bf16[4,128,2048]{2,1,0:T(8,128)(2,1)}), bf16[4,128,2048]{2,1,0:T(8,128)(2,1)}, u32[]{:S(2)}, u32[]{:S(2)}) async-start(bf16[4,128,2048]{2,1,0:T(8,128)(2,1)} %bitcast.71), calls=%async_computation | async-start | bytes 4194304 | tf_op jit(solution)/shard_map/all_to_all | solution.py:30
  19.3 27.4 %copy-start.3 = (bf16[128,2048]{1,0:T(8,128)(2,1)S(1)}, bf16[128,2048]{1,0:T(8,128)(2,1)}, u32[]{:S(2)}) copy-start(bf16[128,2048]{1,0:T(8,128)(2,1)} %param.17) | copy-start | bytes 1572868
  22.0 25.8 %copy-start.6 = (f32[2048]{0:T(1024)S(1)}, f32[2048]{0:T(1024)}, u32[]{:S(2)}) copy-start(f32[2048]{0:T(1024)} %param.18) | copy-start | bytes 24580
  46.8 1.0 copy-start.1
  51.4 64.1 %copy-start.8 = (bf16[1,2048,512]{2,1,0:T(8,128)(2,1)S(1)}, bf16[1,2048,512]{2,1,0:T(8,128)(2,1)}, u32[]{:S(2)}) copy-start(bf16[1,2048,512]{2,1,0:T(8,128)(2,1)} %param.21) | copy-start | bytes 6291460
  113.9 1.3 copy-start.4
  115.2 43.9 %collective-permute-start.5 = (bf16[512,2048]{1,0:T(8,128)(2,1)S(1)}, bf16[512,2048]{1,0:T(8,128)(2,1)S(1)}, u32[]{:S(2)}, u32[]{:S(2)}) collective-permute-start(bf16[512,2048]{1,0:T(8,128)(2,1)S(1)} %bitcast.72), channel_id=1, source_target_pairs={{0,3},{1,2},{2,1},{3,0},{4,5},{5,4},{6,7},{7,6},{8,11},{9,10},{10,... | collective-permute-start | bytes 6291464 | tf_op jit(solution)/shard_map/ppermute | solution.py:14
  115.5 46.6 %collective-permute-start.2 = (bf16[2048,512]{1,0:T(8,128)(2,1)S(1)}, bf16[2048,512]{1,0:T(8,128)(2,1)S(1)}, u32[]{:S(2)}, u32[]{:S(2)}) collective-permute-start(bf16[2048,512]{1,0:T(8,128)(2,1)S(1)} %bitcast.81), channel_id=1, source_target_pairs={{0,1},{1,0},{2,3},{3,2},{4,7},{5,6},{6,5},{7,4},{8,9},{9,8},{10,11... | collective-permute-start | bytes 6291464 | tf_op jit(solution)/shard_map/ppermute | solution.py:14
  116.1 70.5 %collective-permute-start.4 = (bf16[512,2048]{1,0:T(8,128)(2,1)}, bf16[512,2048]{1,0:T(8,128)(2,1)}, u32[]{:S(2)}, u32[]{:S(2)}) collective-permute-start(bf16[512,2048]{1,0:T(8,128)(2,1)} %bitcast.16), channel_id=1, source_target_pairs={{0,1},{1,0},{2,3},{3,2},{4,7},{5,6},{6,5},{7,4},{8,9},{9,8},{10,11... | collective-permute-start | bytes 6291464 | tf_op jit(solution)/shard_map/ppermute | solution.py:14
  118.2 90.9 %collective-permute-start.3 = (bf16[2048,512]{1,0:T(8,128)(2,1)}, bf16[2048,512]{1,0:T(8,128)(2,1)}, u32[]{:S(2)}, u32[]{:S(2)}) collective-permute-start(bf16[2048,512]{1,0:T(8,128)(2,1)} %bitcast.15), channel_id=1, source_target_pairs={{0,1},{1,0},{2,3},{3,2},{4,7},{5,6},{6,5},{7,4},{8,9},{9,8},{10,11... | collective-permute-start | bytes 6291464 | tf_op jit(solution)/shard_map/ppermute | solution.py:14
  159.1 3.0 copy-start.10
  162.1 1.3 copy-start.9
  217.2 4.6 %copy-start.5 = (bf16[1,64,8,2048]{3,2,0,1:T(8,128)(2,1)S(1)}, bf16[1,64,8,2048]{3,2,0,1:T(8,128)(2,1)}, u32[]{:S(2)}) copy-start(bf16[1,64,8,2048]{3,2,0,1:T(8,128)(2,1)} %copy-done.4) | copy-start | bytes 6291460
  217.2 25.5 %collective-permute-start.6 = (bf16[512,2048]{1,0:T(8,128)(2,1)}, bf16[512,2048]{1,0:T(8,128)(2,1)}, u32[]{:S(2)}, u32[]{:S(2)}) collective-permute-start(bf16[512,2048]{1,0:T(8,128)(2,1)} %add_convert_fusion.1), channel_id=1, source_target_pairs={{0,3},{1,2},{2,1},{3,0},{4,5},{5,4},{6,7},{7,6},{8,11},{9,10},{10,... | collective-permute-start | bytes 6291464 | tf_op jit(solution)/shard_map/ppermute | solution.py:14
  249.4 57.2 %all-to-all-start.2 = ((bf16[64,8,2048]{2,1,0:T(8,128)(2,1)}), bf16[64,8,2048]{2,1,0:T(8,128)(2,1)}, u32[]{:S(2)}, u32[]{:S(2)}) async-start(bf16[64,8,2048]{2,1,0:T(8,128)(2,1)} %fusion), calls=%async_computation.2 | async-start | bytes 4194304 | tf_op jit(solution)/shard_map/all_to_all | solution.py:136
  315.2 4.9 %copy-start.2 = (f32[128,2048]{1,0:T(8,128)S(1)}, f32[128,2048]{1,0:T(8,128)}, u32[]{:S(2)}) copy-start(f32[128,2048]{1,0:T(8,128)} %copy-done.1) | copy-start | bytes 3145732
